TPU v7x, 32 devices: a whole 2x2x4 slice. The times are simulated.
32 devices in a mesh: ep: 32 (over z, y, x, core), tp: 1.
Axes of the slice: x: 2, y: 2, z: 4, core: 2. Of those that a mesh axis runs over, the one named last changes fastest.
Arguments:
- tokens: bfloat16 [4096, 2048], P('ep'), may hold values from -6 to 6
- pre_gain: float32 [2048], replicated, may hold values from 0.1 to 1.9
- post_gain: float32 [2048], P('tp'), may hold values from 0.1 to 1.9
- expert_ids: int32 [4096, 2], P('ep'), may hold values from 0 to 31, all different within a row; in each aligned block of 128 rows (0 to 127, 128 to 255, ...) at most 12 rows name the same one
- route_weights: float32 [4096, 2], P('ep'), may hold values from 0.1 to 1
- w_gate: bfloat16 [32, 2048, 512], P('ep', None, 'tp'), may hold values from -0.125 to 0.125
- w_up: bfloat16 [32, 2048, 512], P('ep', None, 'tp'), may hold values from -0.125 to 0.125
- w_down: bfloat16 [32, 512, 2048], P('ep', None, 'tp'), may hold values from -0.25 to 0.25
Outputs:
- routed: bfloat16 [4096, 2048], P('ep', 'tp')
Inputs may be any that keep to these rules, and one draw needn't show every extreme that they name: `expert_ids`: each row names 2 different experts. Among the rows of one index of ep (aligned blocks of 128 rows) no expert is named by more than 12 rows, a bound that some block reaches.
All inputs are finite; a program needn't handle non-finite values.
Results may differ from a plain program's by a relative error of at most 0.007.
Values may be sent and summed in bfloat16 or wider, within the bound.
A program may use at most 64 MiB of HBM per device.

v0:
```python
import jax
import jax.numpy as jnp
from jax import lax
from jax.sharding import PartitionSpec as P

epsilon = 1e-06


def per_device(tokens, pre_gain, post_gain, expert_ids, route_weights, w_gate, w_up, w_down):
    tok_rows, row_width = tokens.shape
    pick_count = expert_ids.shape[1]
    ep_count = lax.axis_size("ep")
    local_experts = w_gate.shape[0]
    experts = ep_count * local_experts
    capacity = 3 * tok_rows * pick_count // (2 * experts)
    pick_total = tok_rows * pick_count
    flat_ids = expert_ids.reshape(pick_total)
    onehot = (flat_ids[:, None] == jnp.arange(experts, dtype=jnp.int32)[None, :]).astype(
        jnp.bfloat16
    )
    positions = jnp.arange(pick_total, dtype=jnp.int32)
    strict_lower = (positions[None, :] < positions[:, None]).astype(jnp.bfloat16)
    earlier = jnp.dot(strict_lower, onehot, preferred_element_type=jnp.float32)
    slot_index = jnp.sum(earlier * onehot, axis=1).astype(jnp.int32)
    target = flat_ids * capacity + slot_index
    values = tokens.astype(jnp.float32)
    row_scale = lax.rsqrt(jnp.mean(values * values, axis=1, keepdims=True) + epsilon)
    normed = (values * row_scale * pre_gain[None, :]).astype(jnp.bfloat16)
    sent_width = normed.shape[1]
    copies = jnp.broadcast_to(normed[:, None, :], (tok_rows, pick_count, sent_width)).reshape(
        pick_total, sent_width
    )
    buffer = jnp.zeros((experts * capacity, sent_width), jnp.bfloat16).at[target].set(copies)
    arrived = lax.all_to_all(buffer, "ep", split_axis=0, concat_axis=0, tiled=True)
    rows_in = arrived.reshape(ep_count, local_experts, capacity, row_width)
    gate_sum = jnp.einsum("sxcd,xdf->sxcf", rows_in, w_gate, preferred_element_type=jnp.float32)
    up_sum = jnp.einsum("sxcd,xdf->sxcf", rows_in, w_up, preferred_element_type=jnp.float32)
    hidden = (jax.nn.silu(gate_sum) * up_sum).astype(jnp.bfloat16)
    out_cols = w_down.shape[2]
    produced = jnp.einsum(
        "sxcf,xfd->sxcd",
        lax.all_gather(hidden, "tp", axis=3, tiled=True),
        w_down,
        preferred_element_type=jnp.float32,
    )
    results = produced.astype(jnp.bfloat16).reshape(experts * capacity, out_cols)
    returned = lax.all_to_all(results, "ep", split_axis=0, concat_axis=0, tiled=True)
    picked = returned[target].astype(jnp.float32) * route_weights.reshape(pick_total)[:, None]
    mixed = jnp.sum(picked.reshape(tok_rows, pick_count, out_cols), axis=1)
    squares = lax.psum(jnp.sum(mixed * mixed, axis=1), "tp")
    out_scale = lax.rsqrt(squares / row_width + epsilon)
    return (mixed * out_scale[:, None] * post_gain[None, :]).astype(jnp.bfloat16)


def solution(mesh):
    placed = (
        P("ep", None),
        P(),
        P("tp"),
        P("ep", None),
        P("ep", None),
        P("ep", None, "tp"),
        P("ep", None, "tp"),
        P("ep", None, "tp"),
    )
    return jax.shard_map(
        per_device, mesh=mesh, in_specs=placed, out_specs=P("ep", "tp"), check_vma=False
    )
```

profile of v0, /device:TPU:0, one launch (start us, length us, event | category | flops | bytes accessed | tf_op | source)
XLA Modules:
  0.0 150.3 jit_solution(90630593118681558)
XLA Ops:
  0.0 0.0 copy-start
  0.0 0.9 copy.16
  0.9 0.7 broadcast_multiply_fusion
  1.6 0.1 eq.15
  1.8 0.2 fusion.22
  2.0 0.1 copy.15
  2.1 0.1 mul.75
  2.2 1.2 fusion.23
  3.5 1.2 fusion.25
  4.7 0.6 broadcast_in_dim.5
  5.3 1.2 reshape.109
  6.6 4.1 %scatter_custom_fusion = bf16[384,2048]{1,0:T(8,128)(2,1)} fusion(s32[256]{0:T(256)S(1)} %bitcast.50, bf16[256,2048]{1,0:T(8,128)(2,1)} %reshape.109, bf16[]{:T(256)} %constant.8.clone.1), kind=kCustom, calls=%fused_computation.30 | custom fusion | bytes 1573376 | tf_op jit(solution)/shard_map/scatter | solution.py:33
  10.7 3.6 %all_to_all.12 = bf16[32,12,2048]{2,1,0:T(8,128)(2,1)} reshape(bf16[384,2048]{1,0:T(8,128)(2,1)} %scatter_custom_fusion) | data formatting | bytes 3145728 | tf_op jit(solution)/shard_map/all_to_all | solution.py:34
  14.3 0.0 copy-start.4
  14.3 56.0 %all_to_all.18 = bf16[32,12,2048]{2,1,0:T(8,128)(2,1)S(1)} all-to-all(bf16[32,12,2048]{2,1,0:T(8,128)(2,1)} %all_to_all.12), channel_id=1, replica_groups=mesh['ep'=32,'tp'=1] {'ep'}, dimensions={0} | all-to-all | bytes 3145728 | tf_op jit(solution)/shard_map/all_to_all | solution.py:34
  70.3 0.0 copy-start.1
  70.3 1.3 copy-done.1
  71.6 0.0 copy-done.4
  71.6 1.1 fusion.5
  72.7 0.0 copy-done
  72.7 5.4 %convolution_convert_fusion = bf16[32,12,2048]{2,0,1:T(8,128)(2,1)} fusion(bf16[1,512,2048]{2,1,0:T(8,128)(2,1)S(1)} %copy-done, bf16[1,2048,512]{2,1,0:T(8,128)(2,1)} %param.14, bf16[32,12,2048]{2,1,0:T(8,128)(2,1)} %copy-done.1, f32[32,1,12,512]{3,0,2,1:T(8,128)S(1)} %fusion.5), kind=kOutput, calls=%fused_computation.2 | convolution fusion | flops 1612578816 | bytes 8126464 | tf_op jit(solution)/shard_map/sxcf,xfd->sxcd/dot_general | solution.py:40
  78.1 3.6 %copy.19 = bf16[32,12,2048]{2,1,0:T(8,128)(2,1)} copy(bf16[32,12,2048]{2,0,1:T(8,128)(2,1)} %convolution_convert_fusion) | data formatting | bytes 3145728 | tf_op jit(solution)/shard_map/convert_element_type | solution.py:46
  81.7 0.0 copy-start.3
  81.7 4.0 %all-to-all-start.1 = ((bf16[32,12,2048]{2,1,0:T(8,128)(2,1)}), bf16[32,12,2048]{2,1,0:T(8,128)(2,1)}, u32[]{:S(2)}, u32[]{:S(2)}) async-start(bf16[32,12,2048]{2,1,0:T(8,128)(2,1)} %copy.19), calls=%async_computation.1 | async-start | bytes 4194304 | tf_op jit(solution)/shard_map/all_to_all | solution.py:47
  85.7 0.0 copy-done.3
  85.7 0.1 copy.20
  85.9 48.5 %all-to-all-done.1 = bf16[32,12,2048]{2,1,0:T(8,128)(2,1)} async-done(((bf16[32,12,2048]{2,1,0:T(8,128)(2,1)}), bf16[32,12,2048]{2,1,0:T(8,128)(2,1)}, u32[]{:S(2)}, u32[]{:S(2)}) %all-to-all-start.1) | async-done | bytes 1572896 | tf_op jit(solution)/shard_map/all_to_all | solution.py:47
  134.4 3.6 %all_to_all.15 = bf16[384,2048]{1,0:T(8,128)(2,1)} reshape(bf16[32,12,2048]{2,1,0:T(8,128)(2,1)} %all-to-all-done.1) | data formatting | bytes 3145728 | tf_op jit(solution)/shard_map/all_to_all | solution.py:47
  138.0 4.0 %gather_fusion = bf16[256,2048]{1,0:T(8,128)(2,1)S(1)} fusion(bf16[384,2048]{1,0:T(8,128)(2,1)} %all_to_all.15, s32[1024]{0:T(1024)S(1)} %pad_clamp_fusion), kind=kCustom, calls=%fused_computation | custom fusion | bytes 2098176 | tf_op jit(solution)/shard_map/gather | solution.py:48
  142.0 2.4 %reshape.96 = f32[128,2,2048]{2,1,0:T(2,128)} reshape(bf16[256,2048]{1,0:T(8,128)(2,1)S(1)} %gather_fusion) | data formatting | bytes 3145728 | tf_op jit(solution)/shard_map/convert_element_type | solution.py:48
  144.3 0.0 copy-start.2
  144.4 4.8 %multiply_reduce_fusion = f32[128,2048]{1,0:T(8,128)S(1)} fusion(f32[128,2,2048]{2,1,0:T(2,128)} %reshape.96, f32[128,2]{1,0:T(8,128)S(1)} %copy.20), kind=kLoop, calls=%fused_computation.8 | loop fusion | flops 786432 | bytes 3146752 | tf_op jit(solution)/shard_map/reduce_sum | solution.py:49
  149.2 0.2 multiply_reduce_fusion.1
  149.3 0.0 copy-done.2
  149.3 1.0 multiply_convert_fusion
  (5 shorter events, 0.0 us)
Async XLA Ops:
  0.0 72.7 %copy-start = (bf16[1,512,2048]{2,1,0:T(8,128)(2,1)S(1)}, bf16[1,512,2048]{2,1,0:T(8,128)(2,1)}, u32[]{:S(2)}) copy-start(bf16[1,512,2048]{2,1,0:T(8,128)(2,1)} %param.15) | copy-start | bytes 6291460
  14.3 57.3 %copy-start.4 = (bf16[1,2048,512]{2,1,0:T(8,128)(2,1)S(1)}, bf16[1,2048,512]{2,1,0:T(8,128)(2,1)}, u32[]{:S(2)}) copy-start(bf16[1,2048,512]{2,1,0:T(8,128)(2,1)} %param.13) | copy-start | bytes 6291460
  70.3 1.3 copy-start.1
  81.7 4.0 %copy-start.3 = (f32[128,2]{0,1:T(2,128)S(1)}, f32[128,2]{0,1:T(2,128)}, u32[]{:S(2)}) copy-start(f32[128,2]{0,1:T(2,128)} %param.12) | copy-start | bytes 3076
  81.7 52.7 %all-to-all-start.1 = ((bf16[32,12,2048]{2,1,0:T(8,128)(2,1)}), bf16[32,12,2048]{2,1,0:T(8,128)(2,1)}, u32[]{:S(2)}, u32[]{:S(2)}) async-start(bf16[32,12,2048]{2,1,0:T(8,128)(2,1)} %copy.19), calls=%async_computation.1 | async-start | bytes 4194304 | tf_op jit(solution)/shard_map/all_to_all | solution.py:47
  144.3 5.0 %copy-start.2 = (f32[2048]{0:T(1024)S(1)}, f32[2048]{0:T(1024)}, u32[]{:S(2)}) copy-start(f32[2048]{0:T(1024)} %param.10) | copy-start | bytes 24580
where the time goes:
time: 151 us; the launch traced here: 150 us
  blocking collectives  56 us (37%)
  waiting for transfers between devices  48.5 us (32%)
  local copies, waits for them, and re-layouts  25.9 us (17%)
  other arithmetic  9.1 us (6%)
  matrix products  6.72 us (4%)
  starting transfers between devices  3.99 us (3%)
    all_to_all x1, blocking collectives, per_device(): lax.all_to_all(buffer, 'ep', split_axis=0, concat_axis=0, tiled=True)  56 us
    all_to_all x1, waiting for transfers between devices, per_device(): lax.all_to_all(results, 'ep', split_axis=0, concat_axis=0, tiled=True)  48.5 us
    dot_general x1, matrix products, per_device(): jnp.einsum('sxcf,xfd->sxcd', lax.all_gather(hidden, 'tp', axis=3, tiled=T...  5.43 us
    reduce_sum x1, other arithmetic, per_device(): mixed = jnp.sum(picked.reshape(tok_rows, pick_count, out_cols), axis=1)  4.81 us
    scatter x1, local copies, waits for them, and re-layouts, per_device(): jnp.zeros((experts * capacity, sent_width), jnp.bfloat16).at[target]  4.11 us
    all_to_all x1, starting transfers between devices, per_device(): lax.all_to_all(results, 'ep', split_axis=0, concat_axis=0, tiled=True)  3.99 us
    gather x1, local copies, waits for them, and re-layouts, per_device(): returned[target].astype(jnp.float32)  3.97 us
    all_to_all x1, local copies, waits for them, and re-layouts, per_device(): lax.all_to_all(results, 'ep', split_axis=0, concat_axis=0, tiled=True)  3.61 us
  transfers between devices with their start and end apart: 1, of which 1 were waited for; matrix products, arithmetic and copies ran while one was open for 0% of the time, Pallas kernels for 0%

commit v1 on v0

--- a/solution.py
+++ b/solution.py
@@ -1,9 +1,253 @@
+import functools
 import jax
 import jax.numpy as jnp
 from jax import lax
+from jax.experimental import pallas as pl
+from jax.experimental.pallas import tpu as pltpu
 from jax.sharding import PartitionSpec as P
 
 epsilon = 1e-06
+CUTS = 4
+GROUP = 4
+
+
+def fused_kernel(
+    n, cap, tok_ref, pre_ref, post_ref, ids_ref, rw_ref, wg_hbm, wu_hbm, wd_hbm, out_ref,
+    wg, wu, wd, normed, out_buf, in_buf, res_buf, ret_buf, perm, mixed,
+    wsem, send1, recv1, send2, recv2,
+):
+    rows, width = tok_ref.shape
+    part = width // CUTS
+    block = CUTS * cap
+    gb = GROUP * block
+    gc = GROUP * cap
+    groups = n // GROUP
+    side = groups // 2
+    me = lax.axis_index("ep")
+    tp = lax.axis_index("tp")
+    mg = me // GROUP
+    half = mg // side
+    spot = mg % side
+
+    weights = [
+        pltpu.make_async_copy(a.at[0], b, wsem.at[i])
+        for i, (a, b) in enumerate(((wg_hbm, wg), (wu_hbm, wu), (wd_hbm, wd)))
+    ]
+    for w in weights:
+        w.start()
+
+    barrier = pltpu.get_barrier_semaphore()
+
+    def greet(i, c):
+        peer = (me + i) % n
+        pl.semaphore_signal(barrier, inc=1, device_id=(peer, tp), device_id_type=pl.DeviceIdType.MESH)
+        return c
+
+    lax.fori_loop(1, n, greet, 0)
+
+    values = tok_ref[...].astype(jnp.float32)
+    scale = lax.rsqrt(jnp.mean(values * values, axis=1, keepdims=True) + epsilon)
+    normed[...] = (values * scale * pre_ref[...]).astype(jnp.bfloat16)
+
+    lanes = max(128, n)
+    expert = lax.broadcasted_iota(jnp.int32, (rows, lanes), 1)
+    ids0 = ids_ref[:, 0:1]
+    ids1 = ids_ref[:, 1:2]
+    hot0 = (ids0 == expert).astype(jnp.float32)
+    hot1 = (ids1 == expert).astype(jnp.float32)
+    tri = (
+        lax.broadcasted_iota(jnp.int32, (rows, rows), 1)
+        < lax.broadcasted_iota(jnp.int32, (rows, rows), 0)
+    ).astype(jnp.bfloat16)
+    earlier = jnp.dot(tri, (hot0 + hot1).astype(jnp.bfloat16), preferred_element_type=jnp.float32)
+    target0 = ids0.astype(jnp.float32) * cap + jnp.sum(earlier * hot0, axis=1, keepdims=True)
+    target1 = ids1.astype(jnp.float32) * cap + jnp.sum(earlier * hot1, axis=1, keepdims=True)
+    lane = lax.broadcasted_iota(jnp.int32, (rows, rows), 1)
+    flipped = jnp.where(lane == 0, target0, jnp.where(lane == 1, target1, -1.0)).T
+    trow0 = flipped[0:1, :].astype(jnp.int32)
+    trow1 = flipped[1:2, :].astype(jnp.int32)
+    tcol = jnp.concatenate([target0, target1], axis=0).astype(jnp.int32)
+
+    u = lax.broadcasted_iota(jnp.int32, (gb, gb), 0)
+    v = lax.broadcasted_iota(jnp.int32, (gb, gb), 1)
+    vu = (v % block) // cap * gc + v // block * cap + v % cap
+    perm[...] = (u == vu).astype(jnp.bfloat16)
+
+    wrow = lax.broadcasted_iota(jnp.int32, (gb, rows), 0)
+    wslot = wrow // block * cap + wrow % cap
+    wcut = (lax.broadcasted_iota(jnp.int32, (gb, part), 0) % block) // cap
+
+    def span(start, size):
+        return pl.ds(pl.multiple_of(start, size), size)
+
+    def give(peer):
+        return pltpu.make_async_remote_copy(
+            src_ref=out_buf.at[span(peer * block, block)],
+            dst_ref=in_buf.at[span(me * block, block)],
+            send_sem=send1.at[peer], recv_sem=recv1.at[me],
+            device_id=(peer, tp), device_id_type=pl.DeviceIdType.MESH,
+        )
+
+    def take(peer):
+        return pltpu.make_async_remote_copy(
+            src_ref=out_buf.at[span(peer * block, block)],
+            dst_ref=in_buf.at[span(peer * block, block)],
+            send_sem=send1.at[peer], recv_sem=recv1.at[peer],
+            device_id=(peer, tp), device_id_type=pl.DeviceIdType.MESH,
+        )
+
+    def give_back(peer):
+        return pltpu.make_async_remote_copy(
+            src_ref=res_buf.at[span(peer * block, block)],
+            dst_ref=ret_buf.at[span(me * block, block)],
+            send_sem=send2.at[peer], recv_sem=recv2.at[me],
+            device_id=(peer, tp), device_id_type=pl.DeviceIdType.MESH,
+        )
+
+    def take_back(peer):
+        return pltpu.make_async_remote_copy(
+            src_ref=res_buf.at[span(peer * block, block)],
+            dst_ref=ret_buf.at[span(peer * block, block)],
+            send_sem=send2.at[peer], recv_sem=recv2.at[peer],
+            device_id=(peer, tp), device_id_type=pl.DeviceIdType.MESH,
+        )
+
+    def each(g, do):
+        def one(j, c):
+            peer = g * GROUP + (me + j) % GROUP
+
+            @pl.when(peer != me)
+            def _():
+                do(peer)
+
+            return c
+
+        lax.fori_loop(0, GROUP, one, 0)
+
+    def far(i, sign):
+        return (1 - half) * side + (spot + side + sign * i) % side
+
+    def near(i, sign):
+        return half * side + (spot + side + sign * i) % side
+
+    def dispatch(g):
+        want = wslot + g * gc
+        pick = ((trow0 == want) | (trow1 == want)).astype(jnp.bfloat16)
+        spread = jnp.dot(pick, normed[...], preferred_element_type=jnp.float32)
+        chosen = spread[:, 0:part]
+        for q in range(1, CUTS):
+            chosen = jnp.where(wcut == q, spread[:, q * part:(q + 1) * part], chosen)
+        out_buf[span(g * gb, gb), :] = chosen.astype(jnp.bfloat16)
+
+    pl.semaphore_wait(barrier, n - 1)
+
+    def send_step(i, c):
+        for which in (far, near):
+            g = which(i, 1)
+            dispatch(g)
+            each(g, lambda peer: give(peer).start())
+        return c
+
+    lax.fori_loop(0, side, send_step, 0)
+    mine = span(me * block, block)
+    in_buf[mine, :] = out_buf[mine, :]
+    for w in weights:
+        w.wait()
+
+    def experts(g):
+        each(g, lambda peer: take(peer).wait_recv())
+        here = span(g * gb, gb)
+        stacked = jnp.dot(perm[...], in_buf[here, :], preferred_element_type=jnp.float32).astype(jnp.bfloat16)
+        x = jnp.concatenate([stacked[q * gc:(q + 1) * gc, :] for q in range(CUTS)], axis=1)
+        gate = jnp.dot(x, wg[...], preferred_element_type=jnp.float32)
+        up = jnp.dot(x, wu[...], preferred_element_type=jnp.float32)
+        hidden = (gate / (1.0 + jnp.exp(-gate)) * up).astype(jnp.bfloat16)
+        y = jnp.dot(hidden, wd[...], preferred_element_type=jnp.float32).astype(jnp.bfloat16)
+        back = jnp.concatenate([y[:, q * part:(q + 1) * part] for q in range(CUTS)], axis=0)
+        wire = lax.dot_general(perm[...], back, (((0,), (0,)), ((), ())), preferred_element_type=jnp.float32)
+        res_buf[here, :] = wire.astype(jnp.bfloat16)
+        each(g, lambda peer: give_back(peer).start())
+
+    def expert_step(i, c):
+        experts(near(i, -1))
+        experts(far(i, -1))
+        return c
+
+    lax.fori_loop(0, side, expert_step, 0)
+    ret_buf[mine, :] = res_buf[mine, :]
+
+    w0 = rw_ref[:, 0:1]
+    w1 = rw_ref[:, 1:2]
+    mixed[...] = jnp.zeros_like(mixed)
+    pcol = lax.broadcasted_iota(jnp.int32, (2 * rows, gc), 1)
+
+    def combine(g):
+        each(g, lambda peer: take_back(peer).wait_recv())
+        stacked = jnp.dot(
+            perm[...], ret_buf[span(g * gb, gb), :], preferred_element_type=jnp.float32
+        ).astype(jnp.bfloat16)
+        z = jnp.concatenate([stacked[q * gc:(q + 1) * gc, :] for q in range(CUTS)], axis=1)
+        pick = (tcol == pcol + g * gc).astype(jnp.bfloat16)
+        got = jnp.dot(pick, z, preferred_element_type=jnp.float32)
+        mixed[...] += got[:rows] * w0 + got[rows:] * w1
+
+    def near_step(i, c):
+        combine(near(i, 1))
+        return c
+
+    def far_step(i, c):
+        combine(far(i, 1))
+        return c
+
+    lax.fori_loop(0, side, near_step, 0)
+    lax.fori_loop(0, side, far_step, 0)
+
+    total = mixed[...]
+    out_scale = lax.rsqrt(jnp.mean(total * total, axis=1, keepdims=True) + epsilon)
+    out_ref[...] = (total * out_scale * post_ref[...]).astype(jnp.bfloat16)
+
+    def drain(i, c):
+        peer = (me + i) % n
+        give(peer).wait_send()
+        give_back(peer).wait_send()
+        return c
+
+    lax.fori_loop(1, n, drain, 0)
+
+
+def fused(n, cap, tokens, pre_gain, post_gain, expert_ids, route_weights, w_gate, w_up, w_down):
+    rows, width = tokens.shape
+    hidden = w_gate.shape[2]
+    part = width // CUTS
+    block = CUTS * cap
+    gb = GROUP * block
+    vmem = pl.BlockSpec(memory_space=pltpu.VMEM)
+    hbm = pl.BlockSpec(memory_space=pl.ANY)
+    buf = pltpu.VMEM((n * block, part), jnp.bfloat16)
+    return pl.pallas_call(
+        functools.partial(fused_kernel, n, cap),
+        out_shape=jax.ShapeDtypeStruct((rows, width), jnp.bfloat16),
+        in_specs=[vmem] * 5 + [hbm] * 3,
+        out_specs=vmem,
+        scratch_shapes=[
+            pltpu.VMEM((width, hidden), jnp.bfloat16),
+            pltpu.VMEM((width, hidden), jnp.bfloat16),
+            pltpu.VMEM((hidden, width), jnp.bfloat16),
+            pltpu.VMEM((rows, width), jnp.bfloat16),
+            buf, buf, buf, buf,
+            pltpu.VMEM((gb, gb), jnp.bfloat16),
+            pltpu.VMEM((rows, width), jnp.float32),
+            pltpu.SemaphoreType.DMA((3,)),
+            pltpu.SemaphoreType.DMA((n,)),
+            pltpu.SemaphoreType.DMA((n,)),
+            pltpu.SemaphoreType.DMA((n,)),
+            pltpu.SemaphoreType.DMA((n,)),
+        ],
+        compiler_params=pltpu.CompilerParams(collective_id=0, has_side_effects=True),
+    )(
+        tokens, pre_gain.reshape(1, width), post_gain.reshape(1, width), expert_ids, route_weights,
+        w_gate, w_up, w_down,
+    )
 
 
 def per_device(tokens, pre_gain, post_gain, expert_ids, route_weights, w_gate, w_up, w_down):
@@ -52,6 +296,20 @@
     return (mixed * out_scale[:, None] * post_gain[None, :]).astype(jnp.bfloat16)
 
 
+def per_shard(n, tp, tokens, *rest):
+    pre_gain, post_gain, expert_ids, route_weights, w_gate, w_up, w_down = rest
+    rows, width = tokens.shape
+    picks = expert_ids.shape[1]
+    cap = 3 * rows * picks // (2 * n * w_gate.shape[0])
+    fits = (
+        tp == 1 and picks == 2 and w_gate.shape[0] == 1 and n % (2 * GROUP) == 0 and n <= 128
+        and rows == 128 and (CUTS * cap) % 16 == 0 and cap > 0 and width % (CUTS * 128) == 0
+    )
+    if fits:
+        return fused(n, cap, tokens, *rest)
+    return per_device(tokens, *rest)
+
+
 def solution(mesh):
     placed = (
         P("ep", None),
@@ -64,5 +322,6 @@
         P("ep", None, "tp"),
     )
     return jax.shard_map(
-        per_device, mesh=mesh, in_specs=placed, out_specs=P("ep", "tp"), check_vma=False
-    )
+        functools.partial(per_shard, mesh.shape["ep"], mesh.shape["tp"]),
+        mesh=mesh, in_specs=placed, out_specs=P("ep", "tp"), check_vma=False,
+    )

time: 151 us -> 84.3 us (0.56)
  Pallas kernels: 0 us -> 79.3 us
  blocking collectives: 56 us -> 0 us
  waiting for transfers between devices: 48.5 us -> 0 us
  local copies, waits for them, and re-layouts: 25.9 us -> 4.7 us
  other arithmetic: 9.1 us -> 0 us
  matrix products: 6.72 us -> 0 us
  starting transfers between devices: 3.99 us -> 0 us
    pallas_call x0 -> x1, Pallas kernels: none -> 79.3 us  [fused(): pl.pallas_call(functools.partial(fused_kernel, n, cap), out_shape=jax.Sha...]
    all_to_all x1 -> x0, blocking collectives: 56 us -> none  [per_device(): lax.all_to_all(buffer, 'ep', split_axis=0, concat_axis=0, tiled=True)]
    all_to_all x1 -> x0, waiting for transfers between devices: 48.5 us -> none  [per_device(): lax.all_to_all(results, 'ep', split_axis=0, concat_axis=0, tiled=True)]
    all_to_all x2 -> x0, local copies, waits for them, and re-layouts: 7.2 us -> none  [the longest x1 3.61 us: per_device(): lax.all_to_all(results, 'ep', split_axis=0, concat_axis=0, tiled=True)]
    dot_general x3 -> x0, matrix products: 6.72 us -> none  [the longest x1 5.43 us: per_device(): jnp.einsum('sxcf,xfd->sxcd', lax.all_gather(hidden, 'tp', axis=3, tiled=T...]
    reduce_sum x3 -> x0, other arithmetic: 6.2 us -> none  [the longest x1 4.81 us: per_device(): mixed = jnp.sum(picked.reshape(tok_rows, pick_count, out_cols), axis=1)]
    convert_element_type x2 -> x0, local copies, waits for them, and re-layouts: 5.97 us -> none  [the longest x1 3.61 us: per_device(): produced.astype(jnp.bfloat16).reshape(experts * capacity, out_cols)]
    scatter x1 -> x0, local copies, waits for them, and re-layouts: 4.11 us -> none  [per_device(): jnp.zeros((experts * capacity, sent_width), jnp.bfloat16).at[target]]
  transfers between devices with their start and end apart: 1 -> 0, of which waited for: 1 -> 0; matrix products, arithmetic and copies ran while one was open for 0% -> 0% of each run, Pallas kernels for 0% -> 0%
where the time goes in v1:
time: 84.3 us; the launch traced here: 84.1 us
  Pallas kernels  79.3 us (94%)
  local copies, waits for them, and re-layouts  4.7 us (6%)
    pallas_call x1, Pallas kernels, fused(): pl.pallas_call(functools.partial(fused_kernel, n, cap), out_shape=jax.Sha...  79.3 us
    unnamed x3, local copies, waits for them, and re-layouts  4.7 us

profile of v1, /device:TPU:0, one launch (start us, length us, event | category | flops | bytes accessed | tf_op | source)
XLA Modules:
  0.0 84.1 jit_solution(13826288023934045496)
XLA Ops:
  0.0 1.4 %copy.9.ids_ref = s32[128,2]{1,0:T(8,128)} copy(s32[128,2]{0,1:T(2,128)} %param.11) | data formatting | bytes 2048 | tf_op args[3]
  1.4 1.4 %copy.10.rw_ref = f32[128,2]{1,0:T(8,128)} copy(f32[128,2]{0,1:T(2,128)} %param.12) | data formatting | bytes 2048 | tf_op args[4]
  2.8 79.3 %shard_map.82 = bf16[128,2048]{1,0:T(8,128)(2,1)} custom-call(bf16[128,2048]{1,0:T(8,128)(2,1)} %tok_ref.1, f32[1,2048]{1,0:T(1,128)} %bitcast.2, f32[1,2048]{1,0:T(1,128)} %bitcast.3, s32[128,2]{1,0:T(8,128)} %copy.9.ids_ref, f32[128,2]{1,0:T(8,128)} %copy.10.rw_ref, bf16[1,2048,512]{2,1,0:T(8,128)(2,1)} %wg_hbm.1, bf16[1,2048,512]{2,1,0:T(8,128)(2,1)} %wu_hbm.1, ...), custom_call_target="tpu_custom_call" | custom-call | tf_op jit(solution)/shard_map/pallas_call | solution.py:227
  82.2 1.9 %copy.12 = bf16[128,2048]{1,0:T(8,128)(2,1)} copy(bf16[128,2048]{1,0:T(8,128)(2,1)} %shard_map.82) | data formatting | bytes 1048576

commit v2 on v1

v2 whole, which is shorter than its diff:
```python
import functools
import jax
import jax.numpy as jnp
from jax import lax
from jax.experimental import pallas as pl
from jax.experimental.pallas import tpu as pltpu
from jax.sharding import PartitionSpec as P

epsilon = 1e-06
CUTS = 4
GROUP = 4
EARLY = 2


def fused_kernel(
    n, cap, tok_ref, pre_ref, post_ref, ids_ref, rw_ref, wg_hbm, wu_hbm, wd_hbm, out_ref,
    wg, wu, wd, toks, meta, part_out, part_in, out_buf, in_buf, res_buf, ret_buf, perm, mixed,
    wsem, send1, recv1, send2, recv2, xsend, xrecv,
):
    rows, width = tok_ref.shape
    part = width // CUTS
    block = CUTS * cap
    gb = GROUP * block
    gc = GROUP * cap
    groups = n // GROUP
    side = groups // 2
    quarter = n // 4
    gq = groups // 4
    me = lax.axis_index("ep")
    tp = lax.axis_index("tp")
    mg = me // GROUP
    half = mg // side
    spot = mg % side
    plane = me // quarter
    is_mid = (plane == 1) | (plane == 2)
    partner = jnp.where(plane == 1, me + quarter, jnp.where(plane == 2, me - quarter, me))
    guest = jnp.where(is_mid, 1, 0)
    other = (me + n // 2) % n
    MESH = pl.DeviceIdType.MESH

    weights = [
        pltpu.make_async_copy(a.at[0], b, wsem.at[i])
        for i, (a, b) in enumerate(((wg_hbm, wg), (wu_hbm, wu), (wd_hbm, wd)))
    ]
    for w in weights:
        w.start()

    barrier = pltpu.get_barrier_semaphore()

    def greet(i, c):
        pl.semaphore_signal(barrier, inc=1, device_id=((me + i) % n, tp), device_id_type=MESH)
        return c

    lax.fori_loop(1, n, greet, 0)

    values = tok_ref[...].astype(jnp.float32)
    scale = lax.rsqrt(jnp.mean(values * values, axis=1, keepdims=True) + epsilon)
    toks[0:rows, :] = (values * scale * pre_ref[...]).astype(jnp.bfloat16)

    sub = lax.broadcasted_iota(jnp.int32, (rows, rows), 0)
    lane = lax.broadcasted_iota(jnp.int32, (rows, rows), 1)

    def columns(four):
        spread = jnp.where(sub == 3, four[3], 0.0)
        for i in range(3):
            spread = jnp.where(sub == i, four[i], spread)
        turned = spread.T
        return [turned[:, i:i + 1] for i in range(4)]

    w0row, w1row = rw_ref[0:1, :], rw_ref[1:2, :]
    ids0, ids1, _, _ = columns(
        [ids_ref[0:1, :].astype(jnp.float32), ids_ref[1:2, :].astype(jnp.float32), w0row, w1row]
    )
    expert = lane.astype(jnp.float32)
    hot0 = (ids0 == expert).astype(jnp.float32)
    hot1 = (ids1 == expert).astype(jnp.float32)
    tri = (lane < sub).astype(jnp.bfloat16)
    earlier = jnp.dot(tri, (hot0 + hot1).astype(jnp.bfloat16), preferred_element_type=jnp.float32)
    target0 = ids0 * cap + jnp.sum(earlier * hot0, axis=1, keepdims=True)
    target1 = ids1 * cap + jnp.sum(earlier * hot1, axis=1, keepdims=True)
    flipped = jnp.where(lane == 0, target0, jnp.where(lane == 1, target1, -1.0)).T
    eight = lax.broadcasted_iota(jnp.int32, (8, rows), 0)
    table = jnp.where(eight == 0, flipped[0:1, :], jnp.where(eight == 1, flipped[1:2, :], 0.0))
    meta[0:8, :] = jnp.where(eight == 2, w0row, jnp.where(eight == 3, w1row, table))

    def span(start, size):
        return pl.ds(pl.multiple_of(start, size), size)

    def swap(i, src, dst):
        return pltpu.make_async_remote_copy(
            src_ref=src, dst_ref=dst, send_sem=xsend.at[i], recv_sem=xrecv.at[i],
            device_id=(partner, tp), device_id_type=MESH,
        )

    swaps = [
        swap(0, meta.at[pl.ds(0, 8)], meta.at[pl.ds(8, 8)]),
        swap(1, toks.at[pl.ds(0, rows)], toks.at[pl.ds(rows, rows)]),
        swap(2, part_out, part_in),
    ]

    pl.semaphore_wait(barrier, n - 1)

    @pl.when(is_mid)
    def _():
        swaps[0].start()
        swaps[1].start()

    u = lax.broadcasted_iota(jnp.int32, (gb, gb), 0)
    v = lax.broadcasted_iota(jnp.int32, (gb, gb), 1)
    vu = (v % block) // cap * gc + v // block * cap + v % cap
    perm[...] = (u == vu).astype(jnp.bfloat16)

    wrow = lax.broadcasted_iota(jnp.int32, (gb, rows), 0)
    wslot = wrow // block * cap + wrow % cap
    wcut = (lax.broadcasted_iota(jnp.int32, (gb, part), 0) % block) // cap

    def relayed(slot):
        return is_mid & (slot // (n // 2) != half)

    def target_of(slot):
        return jnp.where(relayed(slot), (slot + n // 2) % n, slot)

    def guested(s):
        q = s // quarter
        return ((q == 1) | (q == 2)) & (s // (n // 2) != half)

    def carrier(s):
        q = s // quarter
        return jnp.where(guested(s), jnp.where(q == 1, s + quarter, s - quarter), s)

    def give(slot):
        source = jnp.where(relayed(slot), partner, me)
        return pltpu.make_async_remote_copy(
            src_ref=out_buf.at[span(slot * block, block)],
            dst_ref=in_buf.at[span(source * block, block)],
            send_sem=send1.at[slot], recv_sem=recv1.at[source],
            device_id=(target_of(slot), tp), device_id_type=MESH,
        )

    def take(s):
        return pltpu.make_async_remote_copy(
            src_ref=out_buf.at[span(s * block, block)],
            dst_ref=in_buf.at[span(s * block, block)],
            send_sem=send1.at[s], recv_sem=recv1.at[s],
            device_id=(carrier(s), tp), device_id_type=MESH,
        )

    def give_back(s):
        slot = jnp.where(guested(s), other, me)
        return pltpu.make_async_remote_copy(
            src_ref=res_buf.at[span(s * block, block)],
            dst_ref=ret_buf.at[span(slot * block, block)],
            send_sem=send2.at[s], recv_sem=recv2.at[slot],
            device_id=(carrier(s), tp), device_id_type=MESH,
        )

    def take_back(slot):
        return pltpu.make_async_remote_copy(
            src_ref=res_buf.at[span(slot * block, block)],
            dst_ref=ret_buf.at[span(slot * block, block)],
            send_sem=send2.at[slot], recv_sem=recv2.at[slot],
            device_id=(target_of(slot), tp), device_id_type=MESH,
        )

    def each(g, device, do):
        def one(j, c):
            index = g * GROUP + (me + j) % GROUP

            @pl.when(device(index) != me)
            def _():
                do(index)

            return c

        lax.fori_loop(0, GROUP, one, 0)

    def far(i, sign):
        return (1 - half) * side + (spot + side + sign * i) % side

    def near(i, sign):
        return half * side + (spot + side + sign * i) % side

    def dispatch(g, which, real):
        lines = meta[span(which * 8, 8), :]
        want = (wslot + real * gc).astype(jnp.float32)
        pick = ((lines[0:1, :] == want) | (lines[1:2, :] == want)).astype(jnp.bfloat16)
        spread = jnp.dot(pick, toks[span(which * rows, rows), :], preferred_element_type=jnp.float32)
        chosen = spread[:, 0:part]
        for q in range(1, CUTS):
            chosen = jnp.where(wcut == q, spread[:, q * part:(q + 1) * part], chosen)
        out_buf[span(g * gb, gb), :] = chosen.astype(jnp.bfloat16)
        each(g, target_of, lambda slot: give(slot).start())

    def real_group(g):
        return jnp.where(is_mid, (g + side) % groups, g)

    def near_send(i, c):
        g = near(i, 1)
        dispatch(g, 0, g)
        return c

    def far_send(i, c):
        g = far(i, 1)
        dispatch(g, guest, real_group(g))
        return c

    mine = span(me * block, block)
    theirs = span(partner * block, block)
    across = span(other * block, block)

    lax.fori_loop(0, side, near_send, 0)
    in_buf[mine, :] = out_buf[mine, :]

    @pl.when(jnp.logical_not(is_mid))
    def _():
        lax.fori_loop(0, side, far_send, 0)

    for w in weights:
        w.wait()

    def experts(g):
        each(g, carrier, lambda s: take(s).wait_recv())
        here = span(g * gb, gb)
        stacked = jnp.dot(perm[...], in_buf[here, :], preferred_element_type=jnp.float32).astype(jnp.bfloat16)
        x = jnp.concatenate([stacked[q * gc:(q + 1) * gc, :] for q in range(CUTS)], axis=1)
        gate = jnp.dot(x, wg[...], preferred_element_type=jnp.float32)
        up = jnp.dot(x, wu[...], preferred_element_type=jnp.float32)
        hidden = (gate / (1.0 + jnp.exp(-gate)) * up).astype(jnp.bfloat16)
        y = jnp.dot(hidden, wd[...], preferred_element_type=jnp.float32).astype(jnp.bfloat16)
        back = jnp.concatenate([y[:, q * part:(q + 1) * part] for q in range(CUTS)], axis=0)
        wire = lax.dot_general(perm[...], back, (((0,), (0,)), ((), ())), preferred_element_type=jnp.float32)
        res_buf[here, :] = wire.astype(jnp.bfloat16)
        each(g, carrier, lambda s: give_back(s).start())

    def near_experts(i, c):
        experts(near(i, -1))
        return c

    def far_experts(i, c):
        q = jnp.where(i < gq, 2 - half, 3 * (1 - half))
        experts(q * gq + (mg + gq - i % gq) % gq)
        return c

    lax.fori_loop(0, EARLY, near_experts, 0)

    @pl.when(is_mid)
    def _():
        swaps[0].wait_recv()
        swaps[1].wait_recv()
        lax.fori_loop(0, side, far_send, 0)
        in_buf[theirs, :] = out_buf[across, :]

    lax.fori_loop(EARLY, side, near_experts, 0)
    lax.fori_loop(0, side, far_experts, 0)
    ret_buf[mine, :] = res_buf[mine, :]

    pcol = lax.broadcasted_iota(jnp.int32, (rows, gc), 1)

    def combine(first, which, shift):
        lines = meta[span(which * 8, 8), :]
        t0, t1, w0, w1 = columns([lines[i:i + 1, :] for i in range(4)])

        def step(i, c):
            g = first(i, 1)
            each(g, target_of, lambda slot: take_back(slot).wait_recv())
            stacked = jnp.dot(
                perm[...], ret_buf[span(g * gb, gb), :], preferred_element_type=jnp.float32
            ).astype(jnp.bfloat16)
            z = jnp.concatenate([stacked[q * gc:(q + 1) * gc, :] for q in range(CUTS)], axis=1)
            want = (pcol + shift(g) * gc).astype(jnp.float32)
            got0 = jnp.dot((t0 == want).astype(jnp.bfloat16), z, preferred_element_type=jnp.float32)
            got1 = jnp.dot((t1 == want).astype(jnp.bfloat16), z, preferred_element_type=jnp.float32)
            mixed[...] += got0 * w0 + got1 * w1
            return c

        lax.fori_loop(0, side, step, 0)

    mixed[...] = jnp.zeros_like(mixed)

    @pl.when(is_mid)
    def _():
        ret_buf[across, :] = res_buf[theirs, :]
        combine(far, guest, real_group)
        part_out[...] = mixed[...].astype(jnp.bfloat16)
        swaps[2].start()
        mixed[...] = jnp.zeros_like(mixed)

    combine(near, 0, lambda g: g)

    @pl.when(jnp.logical_not(is_mid))
    def _():
        combine(far, guest, real_group)

    @pl.when(is_mid)
    def _():
        swaps[2].wait_recv()
        mixed[...] += part_in[...].astype(jnp.float32)

    total = mixed[...]
    out_scale = lax.rsqrt(jnp.mean(total * total, axis=1, keepdims=True) + epsilon)
    out_ref[...] = (total * out_scale * post_ref[...]).astype(jnp.bfloat16)

    def drain(i, c):
        @pl.when(target_of(i) != me)
        def _():
            give(i).wait_send()

        @pl.when(carrier(i) != me)
        def _():
            give_back(i).wait_send()

        return c

    lax.fori_loop(0, n, drain, 0)

    @pl.when(is_mid)
    def _():
        for s in swaps:
            s.wait_send()


def fused(n, cap, tokens, pre_gain, post_gain, expert_ids, route_weights, w_gate, w_up, w_down):
    rows, width = tokens.shape
    hidden = w_gate.shape[2]
    part = width // CUTS
    block = CUTS * cap
    gb = GROUP * block
    vmem = pl.BlockSpec(memory_space=pltpu.VMEM)
    hbm = pl.BlockSpec(memory_space=pl.ANY)
    buf = pltpu.VMEM((n * block, part), jnp.bfloat16)
    return pl.pallas_call(
        functools.partial(fused_kernel, n, cap),
        out_shape=jax.ShapeDtypeStruct((rows, width), jnp.bfloat16),
        in_specs=[vmem] * 5 + [hbm] * 3,
        out_specs=vmem,
        scratch_shapes=[
            pltpu.VMEM((width, hidden), jnp.bfloat16),
            pltpu.VMEM((width, hidden), jnp.bfloat16),
            pltpu.VMEM((hidden, width), jnp.bfloat16),
            pltpu.VMEM((2 * rows, width), jnp.bfloat16),
            pltpu.VMEM((16, rows), jnp.float32),
            pltpu.VMEM((rows, width), jnp.bfloat16),
            pltpu.VMEM((rows, width), jnp.bfloat16),
            buf, buf, buf, buf,
            pltpu.VMEM((gb, gb), jnp.bfloat16),
            pltpu.VMEM((rows, width), jnp.float32),
            pltpu.SemaphoreType.DMA((3,)),
            pltpu.SemaphoreType.DMA((n,)),
            pltpu.SemaphoreType.DMA((n,)),
            pltpu.SemaphoreType.DMA((n,)),
            pltpu.SemaphoreType.DMA((n,)),
            pltpu.SemaphoreType.DMA((3,)),
            pltpu.SemaphoreType.DMA((3,)),
        ],
        compiler_params=pltpu.CompilerParams(collective_id=0, has_side_effects=True),
    )(
        tokens, pre_gain.reshape(1, width), post_gain.reshape(1, width), expert_ids.T, route_weights.T,
        w_gate, w_up, w_down,
    )


def per_device(tokens, pre_gain, post_gain, expert_ids, route_weights, w_gate, w_up, w_down):
    tok_rows, row_width = tokens.shape
    pick_count = expert_ids.shape[1]
    ep_count = lax.axis_size("ep")
    local_experts = w_gate.shape[0]
    experts = ep_count * local_experts
    capacity = 3 * tok_rows * pick_count // (2 * experts)
    pick_total = tok_rows * pick_count
    flat_ids = expert_ids.reshape(pick_total)
    onehot = (flat_ids[:, None] == jnp.arange(experts, dtype=jnp.int32)[None, :]).astype(
        jnp.bfloat16
    )
    positions = jnp.arange(pick_total, dtype=jnp.int32)
    strict_lower = (positions[None, :] < positions[:, None]).astype(jnp.bfloat16)
    earlier = jnp.dot(strict_lower, onehot, preferred_element_type=jnp.float32)
    slot_index = jnp.sum(earlier * onehot, axis=1).astype(jnp.int32)
    target = flat_ids * capacity + slot_index
    values = tokens.astype(jnp.float32)
    row_scale = lax.rsqrt(jnp.mean(values * values, axis=1, keepdims=True) + epsilon)
    normed = (values * row_scale * pre_gain[None, :]).astype(jnp.bfloat16)
    sent_width = normed.shape[1]
    copies = jnp.broadcast_to(normed[:, None, :], (tok_rows, pick_count, sent_width)).reshape(
        pick_total, sent_width
    )
    buffer = jnp.zeros((experts * capacity, sent_width), jnp.bfloat16).at[target].set(copies)
    arrived = lax.all_to_all(buffer, "ep", split_axis=0, concat_axis=0, tiled=True)
    rows_in = arrived.reshape(ep_count, local_experts, capacity, row_width)
    gate_sum = jnp.einsum("sxcd,xdf->sxcf", rows_in, w_gate, preferred_element_type=jnp.float32)
    up_sum = jnp.einsum("sxcd,xdf->sxcf", rows_in, w_up, preferred_element_type=jnp.float32)
    hidden = (jax.nn.silu(gate_sum) * up_sum).astype(jnp.bfloat16)
    out_cols = w_down.shape[2]
    produced = jnp.einsum(
        "sxcf,xfd->sxcd",
        lax.all_gather(hidden, "tp", axis=3, tiled=True),
        w_down,
        preferred_element_type=jnp.float32,
    )
    results = produced.astype(jnp.bfloat16).reshape(experts * capacity, out_cols)
    returned = lax.all_to_all(results, "ep", split_axis=0, concat_axis=0, tiled=True)
    picked = returned[target].astype(jnp.float32) * route_weights.reshape(pick_total)[:, None]
    mixed = jnp.sum(picked.reshape(tok_rows, pick_count, out_cols), axis=1)
    squares = lax.psum(jnp.sum(mixed * mixed, axis=1), "tp")
    out_scale = lax.rsqrt(squares / row_width + epsilon)
    return (mixed * out_scale[:, None] * post_gain[None, :]).astype(jnp.bfloat16)


def per_shard(n, tp, tokens, *rest):
    pre_gain, post_gain, expert_ids, route_weights, w_gate, w_up, w_down = rest
    rows, width = tokens.shape
    picks = expert_ids.shape[1]
    cap = 3 * rows * picks // (2 * n * w_gate.shape[0])
    fits = (
        tp == 1 and picks == 2 and w_gate.shape[0] == 1 and n % (4 * GROUP) == 0 and n <= 128
        and rows == 128 and (CUTS * cap) % 16 == 0 and cap > 0 and width % (CUTS * 128) == 0
    )
    if fits:
        return fused(n, cap, tokens, *rest)
    return per_device(tokens, *rest)


def solution(mesh):
    placed = (
        P("ep", None),
        P(),
        P("tp"),
        P("ep", None),
        P("ep", None),
        P("ep", None, "tp"),
        P("ep", None, "tp"),
        P("ep", None, "tp"),
    )
    return jax.shard_map(
        functools.partial(per_shard, mesh.shape["ep"], mesh.shape["tp"]),
        mesh=mesh, in_specs=placed, out_specs=P("ep", "tp"), check_vma=False,
    )
```

time: 84.3 us -> 84.8 us (level)
  the two profiles are of different devices: /device:TPU:0 before, /device:TPU:17 now
where the time goes in v2:
time: 84.8 us; the launch traced here: 84.7 us
  Pallas kernels  82.8 us (98%)
  local copies, waits for them, and re-layouts  1.88 us (2%)
    pallas_call x1, Pallas kernels, fused(): pl.pallas_call(functools.partial(fused_kernel, n, cap), out_shape=jax.Sha...  82.8 us
    unnamed x1, local copies, waits for them, and re-layouts  1.88 us

profile of v2, /device:TPU:17, one launch (start us, length us, event | category | flops | bytes accessed | tf_op | source)
XLA Modules:
  0.0 84.7 jit_solution(3470512089881624630)
XLA Ops:
  0.0 82.8 %shard_map.82 = bf16[128,2048]{1,0:T(8,128)(2,1)} custom-call(bf16[128,2048]{1,0:T(8,128)(2,1)} %tok_ref.1, f32[1,2048]{1,0:T(1,128)} %bitcast.4, f32[1,2048]{1,0:T(1,128)} %bitcast.5, s32[2,128]{1,0:T(2,128)} %bitcast.6, f32[2,128]{1,0:T(2,128)} %bitcast.7, bf16[1,2048,512]{2,1,0:T(8,128)(2,1)} %wg_hbm.1, bf16[1,2048,512]{2,1,0:T(8,128)(2,1)} %wu_hbm.1, ...), custom_call_target="tpu_custom_call" | custom-call | tf_op jit(solution)/shard_map/pallas_call | solution.py:331
  82.8 1.9 %copy.10 = bf16[128,2048]{1,0:T(8,128)(2,1)} copy(bf16[128,2048]{1,0:T(8,128)(2,1)} %shard_map.82) | data formatting | bytes 1048576

commit v3 on v2

--- a/solution.py
+++ b/solution.py
@@ -10,6 +10,9 @@
 CUTS = 4
 GROUP = 4
 EARLY = 2
+HELD = 3
+PROMPT = 0
+DEFER = 3
 
 
 def fused_kernel(
@@ -211,12 +214,11 @@
     lax.fori_loop(0, side, near_send, 0)
     in_buf[mine, :] = out_buf[mine, :]
 
-    @pl.when(jnp.logical_not(is_mid))
-    def _():
-        lax.fori_loop(0, side, far_send, 0)
-
     for w in weights:
         w.wait()
+
+    def send_back(g):
+        each(g, carrier, lambda s: give_back(s).start())
 
     def experts(g):
         each(g, carrier, lambda s: take(s).wait_recv())
@@ -230,27 +232,45 @@
         back = jnp.concatenate([y[:, q * part:(q + 1) * part] for q in range(CUTS)], axis=0)
         wire = lax.dot_general(perm[...], back, (((0,), (0,)), ((), ())), preferred_element_type=jnp.float32)
         res_buf[here, :] = wire.astype(jnp.bfloat16)
-        each(g, carrier, lambda s: give_back(s).start())
-
-    def near_experts(i, c):
-        experts(near(i, -1))
-        return c
 
     def far_experts(i, c):
         q = jnp.where(i < gq, 2 - half, 3 * (1 - half))
-        experts(q * gq + (mg + gq - i % gq) % gq)
-        return c
-
-    lax.fori_loop(0, EARLY, near_experts, 0)
-
-    @pl.when(is_mid)
-    def _():
-        swaps[0].wait_recv()
-        swaps[1].wait_recv()
-        lax.fori_loop(0, side, far_send, 0)
-        in_buf[theirs, :] = out_buf[across, :]
-
-    lax.fori_loop(EARLY, side, near_experts, 0)
+        g = q * gq + (mg + gq - i % gq) % gq
+        experts(g)
+        send_back(g)
+
+        @pl.when(i == DEFER)
+        def _():
+            for k in range(PROMPT, side):
+                send_back(near(k, -1))
+
+        return c
+
+    def near_then_swap(i, c):
+        @pl.when(is_mid & (i == EARLY))
+        def _():
+            swaps[0].wait_recv()
+            swaps[1].wait_recv()
+
+        @pl.when(i == jnp.where(is_mid, EARLY, HELD))
+        def _():
+            lax.fori_loop(0, side, far_send, 0)
+
+        @pl.when(is_mid & (i == EARLY))
+        def _():
+            in_buf[theirs, :] = out_buf[across, :]
+
+        @pl.when(i < side)
+        def _():
+            experts(near(i, -1))
+
+            @pl.when(i < PROMPT)
+            def _():
+                send_back(near(i, -1))
+
+        return c
+
+    lax.fori_loop(0, side + 1, near_then_swap, 0)
     lax.fori_loop(0, side, far_experts, 0)
     ret_buf[mine, :] = res_buf[mine, :]
 

time: 84.8 us -> 75 us (0.88)
  the two profiles are of different devices: /device:TPU:17 before, /device:TPU:0 now
where the time goes in v3:
time: 75 us; the launch traced here: 74.6 us
  Pallas kernels  72.7 us (97%)
  local copies, waits for them, and re-layouts  1.88 us (3%)
    pallas_call x1, Pallas kernels, fused(): pl.pallas_call(functools.partial(fused_kernel, n, cap), out_shape=jax.Sha...  72.7 us
    unnamed x1, local copies, waits for them, and re-layouts  1.88 us

profile of v3, /device:TPU:0, one launch (start us, length us, event | category | flops | bytes accessed | tf_op | source)
XLA Modules:
  0.0 74.6 jit_solution(3726758198678685726)
XLA Ops:
  0.0 72.7 %shard_map.82 = bf16[128,2048]{1,0:T(8,128)(2,1)} custom-call(bf16[128,2048]{1,0:T(8,128)(2,1)} %tok_ref.1, f32[1,2048]{1,0:T(1,128)} %bitcast.4, f32[1,2048]{1,0:T(1,128)} %bitcast.5, s32[2,128]{1,0:T(2,128)} %bitcast.6, f32[2,128]{1,0:T(2,128)} %bitcast.7, bf16[1,2048,512]{2,1,0:T(8,128)(2,1)} %wg_hbm.1, bf16[1,2048,512]{2,1,0:T(8,128)(2,1)} %wu_hbm.1, ...), custom_call_target="tpu_custom_call" | custom-call | tf_op jit(solution)/shard_map/pallas_call | solution.py:351
  72.8 1.9 %copy.10 = bf16[128,2048]{1,0:T(8,128)(2,1)} copy(bf16[128,2048]{1,0:T(8,128)(2,1)} %shard_map.82) | data formatting | bytes 1048576

commit v4 on v3

--- a/solution.py
+++ b/solution.py
@@ -10,6 +10,7 @@
 CUTS = 4
 GROUP = 4
 EARLY = 2
+GRANT = 60 * 1024 * 1024
 HELD = 3
 PROMPT = 0
 DEFER = 3
@@ -297,6 +298,15 @@
 
     mixed[...] = jnp.zeros_like(mixed)
 
+    def given(i, c):
+        @pl.when(target_of(i) != me)
+        def _():
+            give(i).wait_send()
+
+        return c
+
+    lax.fori_loop(0, n, given, 0)
+
     @pl.when(is_mid)
     def _():
         ret_buf[across, :] = res_buf[theirs, :]
@@ -321,10 +331,6 @@
     out_ref[...] = (total * out_scale * post_ref[...]).astype(jnp.bfloat16)
 
     def drain(i, c):
-        @pl.when(target_of(i) != me)
-        def _():
-            give(i).wait_send()
-
         @pl.when(carrier(i) != me)
         def _():
             give_back(i).wait_send()
@@ -346,7 +352,7 @@
     block = CUTS * cap
     gb = GROUP * block
     vmem = pl.BlockSpec(memory_space=pltpu.VMEM)
-    hbm = pl.BlockSpec(memory_space=pl.ANY)
+    hbm = pl.BlockSpec(memory_space=pltpu.HBM)
     buf = pltpu.VMEM((n * block, part), jnp.bfloat16)
     return pl.pallas_call(
         functools.partial(fused_kernel, n, cap),
@@ -372,7 +378,9 @@
             pltpu.SemaphoreType.DMA((3,)),
             pltpu.SemaphoreType.DMA((3,)),
         ],
-        compiler_params=pltpu.CompilerParams(collective_id=0, has_side_effects=True),
+        compiler_params=pltpu.CompilerParams(
+            collective_id=0, has_side_effects=True, vmem_limit_bytes=GRANT
+        ),
     )(
         tokens, pre_gain.reshape(1, width), post_gain.reshape(1, width), expert_ids.T, route_weights.T,
         w_gate, w_up, w_down,

time: 75 us -> 74.8 us (level)
  no operation moved by 1% of the time
where the time goes in v4:
time: 74.8 us; the launch traced here: 74.4 us
  Pallas kernels  72.5 us (97%)
  local copies, waits for them, and re-layouts  1.88 us (3%)
    pallas_call x1, Pallas kernels, fused(): pl.pallas_call(functools.partial(fused_kernel, n, cap), out_shape=jax.Sha...  72.5 us
    unnamed x1, local copies, waits for them, and re-layouts  1.88 us

profile of v4, /device:TPU:0, one launch (start us, length us, event | category | flops | bytes accessed | tf_op | source)
XLA Modules:
  0.0 74.4 jit_solution(15987791353778385036)
XLA Ops:
  0.0 72.5 %shard_map.82 = bf16[128,2048]{1,0:T(8,128)(2,1)} custom-call(bf16[128,2048]{1,0:T(8,128)(2,1)} %tok_ref.1, f32[1,2048]{1,0:T(1,128)} %bitcast.4, f32[1,2048]{1,0:T(1,128)} %bitcast.5, s32[2,128]{1,0:T(2,128)} %bitcast.6, f32[2,128]{1,0:T(2,128)} %bitcast.7, bf16[1,2048,512]{2,1,0:T(8,128)(2,1)} %wg_hbm.1, bf16[1,2048,512]{2,1,0:T(8,128)(2,1)} %wu_hbm.1, ...), custom_call_target="tpu_custom_call" | custom-call | tf_op jit(solution)/shard_map/pallas_call | solution.py:357
  72.6 1.9 %copy.10 = bf16[128,2048]{1,0:T(8,128)(2,1)} copy(bf16[128,2048]{1,0:T(8,128)(2,1)} %shard_map.82) | data formatting | bytes 1048576
